TPU v7x, 32 devices: a whole 2x2x4 slice. The times are simulated.
32 devices in a mesh: sp: 8 (over z, x), tp: 4 (over y, core).
Axes of the slice: x: 2, y: 2, z: 4, core: 2. Of those that a mesh axis runs over, the one named last changes fastest.
Arguments:
- stream: bfloat16 [4096, 2048], P(('sp', 'tp')), may hold values from -6 to 6
- projected: bfloat16 [4096, 2048], P('sp', 'tp'), may hold values from -6 to 6
- segments: int32 [4096], P('sp'), may hold values from 0 to 3, never falling along the last dimension, each value on 1 to 1536 neighbouring positions
- group_weight: bfloat16 [4, 512, 512], replicated, may hold values from -0.25 to 0.25
- group_scale: float32 [2048], replicated, may hold values from 0.1 to 1.9
- out_weight: bfloat16 [2048, 2048], replicated, may hold values from -0.125 to 0.125
- ffn_gain: float32 [2048], replicated, may hold values from 0.1 to 1.9
- routes: int32 [4096, 4], P(('sp', 'tp')), may hold values from 0 to 31, all different within a row; in each aligned block of 128 rows (0 to 127, 128 to 255, ...) at most 24 rows name the same one
- route_weights: float32 [4096, 4], P(('sp', 'tp')), may hold values from 0.05 to 0.5
- expert_gate: bfloat16 [32, 2048, 1024], P(('sp', 'tp')), may hold values from -0.25 to 0.25
- expert_up: bfloat16 [32, 2048, 1024], P(('sp', 'tp')), may hold values from -0.25 to 0.25
- expert_down: bfloat16 [32, 1024, 2048], P(('sp', 'tp')), may hold values from -0.1875 to 0.1875
Outputs:
- combined: bfloat16 [4096, 2048], P(('sp', 'tp'))
Inputs may be any that keep to these rules, and one draw needn't show every extreme that they name: `segments`: document numbers never fall along the positions; a document has 1 to 1536 positions, and one has exactly 1536. `routes`: each row names 4 different experts. Among the 128 rows of one device (aligned blocks), no expert is named more than 24 times, and in some blocks one is named exactly 24 times.
All inputs are finite; a program needn't handle non-finite values.
Results may differ from a plain program's by a relative error of at most 0.015.
Values may be sent and summed in bfloat16 or wider, within the bound.
A program may use at most 128 MiB of HBM per device.

v0:
```python
import jax
import jax.numpy as jnp
from jax import lax
from jax.experimental import pallas as pl
from jax.experimental.pallas import tpu as pltpu
from jax.sharding import PartitionSpec as P

GROUPS = 4


norm_eps = 1e-05
clamp_limit = 7.0
sigmoid_alpha = 1.702
longest_window = 16


def pool_kernel(group_width, halo_ref, rows_ref, docs_ref, mixed_ref):
    channels = rows_ref.shape[1]
    first = lax.axis_index("tp") * channels
    docs = docs_ref[...]
    same = [docs == pltpu.roll(docs, 1 << k, 0) for k in range(GROUPS)]
    for lane in range(0, channels, 128):
        cols = slice(lane, lane + 128)
        values = jnp.concatenate([halo_ref[:, cols], rows_ref[:, cols]], 0).astype(jnp.float32)
        total, count = values, jnp.ones_like(values)
        channel = first + lane + lax.broadcasted_iota(jnp.int32, values.shape, 1)
        for k in range(GROUPS):
            joins = same[k] & (channel >= k * group_width)
            total = jnp.where(joins, total + pltpu.roll(total, 1 << k, 0), total)
            count = jnp.where(joins, count + pltpu.roll(count, 1 << k, 0), count)
        mixed_ref[:, cols] = (total / count - values)[longest_window:].astype(jnp.bfloat16)


def pool(projected, segments, group_width):
    sp_count = lax.axis_size("sp")
    row_count, channels = projected.shape
    onward = [(i, i + 1) for i in range(sp_count - 1)]
    halo = lax.ppermute(projected[row_count - longest_window :], "sp", onward)
    halo_docs = lax.ppermute(segments[row_count - longest_window :], "sp", onward)
    halo_docs = jnp.where(lax.axis_index("sp") == 0, -1, halo_docs)
    docs = jnp.concatenate([halo_docs, segments])
    docs = jnp.broadcast_to(docs[:, None], (row_count + longest_window, 128))
    return pl.pallas_call(
        lambda *refs: pool_kernel(group_width, *refs),
        out_shape=jax.ShapeDtypeStruct((row_count, channels), jnp.bfloat16),
        name="pool",
    )(halo, projected, docs)


def slots_of(routes, expert_count, capacity):
    tok_count = routes.shape[0]
    named = routes[:, :, None] == jnp.arange(expert_count, dtype=jnp.int32)
    marks = jnp.sum(named.astype(jnp.float32), 1).astype(jnp.bfloat16)
    at = jnp.arange(tok_count, dtype=jnp.int32)
    earlier = (at[None, :] < at[:, None]).astype(jnp.bfloat16)
    before = jnp.dot(earlier, marks, preferred_element_type=jnp.float32)
    rank = jnp.sum(jnp.where(named, before[:, None, :], 0.0), 2).astype(jnp.int32)
    return routes * capacity + rank


def rms_scale(resid, gain):
    values = resid.astype(jnp.float32)
    inverse = lax.rsqrt(jnp.mean(values * values, -1, keepdims=True) + norm_eps)
    return (values * inverse * gain).astype(jnp.bfloat16)


def mixer(mixed, stream, group_weight, group_scale, out_weight, ffn_gain):
    tokens_here = lax.all_to_all(mixed, "tp", split_axis=0, concat_axis=1, tiled=True)
    group_width = group_weight.shape[1]
    grouped = jnp.concatenate(
        [
            jnp.dot(
                tokens_here[:, g * group_width : (g + 1) * group_width],
                group_weight[g],
                preferred_element_type=jnp.float32,
            )
            for g in range(GROUPS)
        ],
        1,
    )
    scaled = (grouped * group_scale).astype(jnp.bfloat16)
    mixer_out = jnp.dot(scaled, out_weight, preferred_element_type=jnp.float32)
    resid = (stream.astype(jnp.float32) + mixer_out).astype(jnp.bfloat16)
    return resid, rms_scale(resid, ffn_gain)


CHUNKS = 4


def experts_kernel(
    z_count,
    x_count,
    tp_count,
    normed_ref,
    resid_ref,
    select_ref,
    weigh_ref,
    gate_hbm,
    up_hbm,
    down_hbm,
    out_ref,
    gate_ref,
    up_ref,
    down_ref,
    column,
    outgoing,
    rows,
    gate_sum,
    up_sum,
    activated,
    results,
    returned,
    part,
    right_out,
    left_out,
    right_in,
    left_in,
    load_sem,
    col_send,
    col_recv,
    plane_send,
    plane_recv,
    back_send,
    back_recv,
    sum_send,
    sum_recv,
):
    sp, tp = lax.axis_index("sp"), lax.axis_index("tp")
    z, x = lax.div(sp, x_count), lax.rem(sp, x_count)
    plane = x_count * tp_count
    place = x * tp_count + tp
    tok, width = normed_ref.shape
    wide = width // CHUNKS
    share = select_ref.shape[0] // plane
    tile = min(256, wide)
    last = z_count - 1
    has_right, has_left = z < last, z > 0

    def at_z(step):
        return {"sp": sp + step * x_count, "tp": tp}

    def at_plane(other):
        return {"sp": z * x_count + lax.div(other, tp_count), "tp": lax.rem(other, tp_count)}

    def remote(src, dst, send, recv, device):
        return pltpu.make_async_remote_copy(
            src_ref=src,
            dst_ref=dst,
            send_sem=send,
            recv_sem=recv,
            device_id=device,
            device_id_type=pl.DeviceIdType.MESH,
        )

    def cols_of(k):
        return pl.ds(pl.multiple_of(k * wide, wide), wide)

    def share_of(i):
        return pl.ds(pl.multiple_of(i * share, share), share)

    loads = [
        pltpu.make_async_copy(src, dst, load_sem.at[i])
        for i, (src, dst) in enumerate(
            ((gate_hbm, gate_ref), (up_hbm, up_ref), (down_hbm, down_ref))
        )
    ]

    barrier = pltpu.get_barrier_semaphore()

    def greet(device):
        pl.semaphore_signal(barrier, inc=1, device_id=device, device_id_type=pl.DeviceIdType.MESH)

    pl.when(has_right)(lambda: greet(at_z(1)))
    pl.when(has_left)(lambda: greet(at_z(-1)))

    @pl.loop(1, plane)
    def _(i):
        greet(at_plane(lax.rem(place + i, plane)))

    for load in loads:
        load.start()
    gate_sum[...] = jnp.zeros_like(gate_sum)
    up_sum[...] = jnp.zeros_like(up_sum)
    pl.semaphore_wait(
        barrier, plane - 1 + has_right.astype(jnp.int32) + has_left.astype(jnp.int32)
    )

    def to_right(k, e):
        src = normed_ref.at[:, cols_of(k)] if e == 0 else column.at[k, e - 1]
        return remote(
            src, column.at[k, e], col_send.at[k, 0, e], col_recv.at[k, e], at_z(1)
        )

    def to_left(k, e):
        src = normed_ref.at[:, cols_of(k)] if e == 0 else column.at[k, z_count - e - 1]
        back = z_count - e - 2
        return remote(
            src, column.at[k, back], col_send.at[k, 1, e], col_recv.at[k, back], at_z(-1)
        )

    def send_own(k):
        pl.when(has_right)(lambda: to_right(k, 0).start())
        pl.when(has_left)(lambda: to_left(k, 0).start())

    def relay(k):
        for e in range(1, z_count):

            @pl.when(z >= e)
            def _():
                to_right(k, e - 1).wait_recv()
                if e < last:
                    pl.when(has_right)(lambda: to_right(k, e).start())

            @pl.when(last - z >= e)
            def _():
                to_left(k, e - 1).wait_recv()
                if e < last:
                    pl.when(has_left)(lambda: to_left(k, e).start())

    def to_expert(k, i):
        other = lax.rem(place + i, plane)
        return remote(
            outgoing.at[k, share_of(other)],
            rows.at[k, share_of(i)],
            plane_send.at[k, i - 1],
            plane_recv.at[k, i - 1],
            at_plane(other),
        )

    def dispatch(k):
        own = jnp.dot(
            select_ref[:, :tok], normed_ref[:, cols_of(k)], preferred_element_type=jnp.float32
        )
        others = jnp.dot(
            select_ref[:, tok:],
            column[k].reshape(last * tok, wide),
            preferred_element_type=jnp.float32,
        )
        outgoing[k] = (own + others).astype(jnp.bfloat16)

        @pl.loop(1, plane)
        def _(i):
            to_expert(k, i).start()

        rows[k, pl.ds(0, share)] = outgoing[k, share_of(place)]

    def accumulate(k):
        @pl.loop(1, plane)
        def _(i):
            to_expert(k, i).wait_recv()

        @pl.loop(0, gate_ref.shape[1] // tile)
        def _(n):
            cols = pl.ds(pl.multiple_of(n * tile, tile), tile)
            gate_sum[:, cols] += jnp.dot(
                rows[k], gate_ref[cols_of(k), cols], preferred_element_type=jnp.float32
            )
            up_sum[:, cols] += jnp.dot(
                rows[k], up_ref[cols_of(k), cols], preferred_element_type=jnp.float32
            )

    send_own(0)

    @pl.loop(0, CHUNKS)
    def _(k):
        pl.when(k + 1 < CHUNKS)(lambda: send_own(k + 1))
        relay(k)
        dispatch(k)

        @pl.when(k == 1)
        def _():
            loads[0].wait()
            loads[1].wait()

        pl.when(k > 0)(lambda: accumulate(k - 1))

    accumulate(CHUNKS - 1)

    @pl.loop(0, gate_ref.shape[1] // tile)
    def _(n):
        cols = pl.ds(pl.multiple_of(n * tile, tile), tile)
        gated = jnp.minimum(gate_sum[:, cols], clamp_limit)
        linear = jnp.clip(up_sum[:, cols], -clamp_limit, clamp_limit)
        activated[:, cols] = (
            gated * jax.nn.sigmoid(sigmoid_alpha * gated) * (linear + 1.0)
        ).astype(jnp.bfloat16)

    loads[2].wait()

    def to_relay(k, i):
        return remote(
            results.at[k, share_of(i)],
            returned.at[k, share_of(place)],
            back_send.at[k, i - 1],
            back_recv.at[k, i - 1],
            at_plane(lax.rem(place + plane - i, plane)),
        )

    @pl.loop(0, CHUNKS)
    def _(k):
        @pl.loop(0, wide // tile)
        def _(n):
            cols = pl.ds(pl.multiple_of(n * tile, tile), tile)
            from_cols = pl.ds(pl.multiple_of(k * wide + n * tile, tile), tile)
            results[k, :, cols] = jnp.dot(
                activated[...], down_ref[:, from_cols], preferred_element_type=jnp.float32
            ).astype(jnp.bfloat16)

        @pl.loop(1, plane)
        def _(i):
            to_relay(k, i).start()

        returned[k, share_of(place)] = results[k, pl.ds(0, share)]

    def combine(k):
        @pl.loop(1, plane)
        def _(i):
            to_relay(k, i).wait_recv()

        part[k] = jnp.dot(weigh_ref[...], returned[k], preferred_element_type=jnp.float32)

    def sum_right(k, e):
        return remote(
            right_out.at[k, e - 1],
            right_in.at[k, e - 1],
            sum_send.at[k, 0, e - 1],
            sum_recv.at[k, 0, e - 1],
            at_z(1),
        )

    def sum_left(k, e):
        return remote(
            left_out.at[k, e - 1],
            left_in.at[k, e - 1],
            sum_send.at[k, 1, e - 1],
            sum_recv.at[k, 1, e - 1],
            at_z(-1),
        )

    def add_up(k):
        for e in range(last, 0, -1):

            @pl.when(z + e <= last)
            def _():
                mine = slice((z_count - e) * tok, (z_count - e + 1) * tok)
                if e < last:

                    @pl.when(has_left)
                    def _():
                        sum_right(k, e + 1).wait_recv()
                        part[k, mine] += right_in[k, e].astype(jnp.float32)

                right_out[k, e - 1] = part[k, mine].astype(jnp.bfloat16)
                sum_right(k, e).start()

            @pl.when(z >= e)
            def _():
                mine = slice(e * tok, (e + 1) * tok)
                if e < last:

                    @pl.when(has_right)
                    def _():
                        sum_left(k, e + 1).wait_recv()
                        part[k, mine] += left_in[k, e].astype(jnp.float32)

                left_out[k, e - 1] = part[k, mine].astype(jnp.bfloat16)
                sum_left(k, e).start()

    def finish(k):
        own = slice(0, tok)

        @pl.when(has_left)
        def _():
            sum_right(k, 1).wait_recv()
            part[k, own] += right_in[k, 0].astype(jnp.float32)

        @pl.when(has_right)
        def _():
            sum_left(k, 1).wait_recv()
            part[k, own] += left_in[k, 0].astype(jnp.float32)

        out_ref[:, cols_of(k)] = (
            resid_ref[:, cols_of(k)].astype(jnp.float32) + part[k, own]
        ).astype(jnp.bfloat16)

    combine(0)

    @pl.loop(0, CHUNKS)
    def _(k):
        pl.when(k + 1 < CHUNKS)(lambda: combine(k + 1))
        add_up(k)
        pl.when(k > 0)(lambda: finish(k - 1))

    finish(CHUNKS - 1)

    @pl.loop(0, CHUNKS)
    def _(k):
        for e in range(last):

            @pl.when((z >= e) & has_right)
            def _():
                to_right(k, e).wait_send()

            @pl.when((last - z >= e) & has_left)
            def _():
                to_left(k, e).wait_send()

        for e in range(1, z_count):
            pl.when(z + e <= last)(lambda: sum_right(k, e).wait_send())
            pl.when(z >= e)(lambda: sum_left(k, e).wait_send())

        @pl.loop(1, plane)
        def _(i):
            to_expert(k, i).wait_send()
            to_relay(k, i).wait_send()


def run_experts(normed, resid, routes, route_weights, gate, up, down):
    tok, width = normed.shape
    sp_count, tp_count = lax.axis_size("sp"), lax.axis_size("tp")
    x_count = max(tp_count // 2, 1)
    z_count = sp_count // x_count
    plane = x_count * tp_count
    top_count = routes.shape[1]
    hidden = gate.shape[1]
    capacity = 3 * tok * top_count // (2 * plane * z_count)
    share = -(-z_count * capacity // 16) * 16
    slots = slots_of(routes, plane * z_count, capacity)
    info = jnp.concatenate([slots.astype(jnp.float32), route_weights], 1)
    z = lax.axis_index("sp") // x_count
    slot_ids = jnp.arange(plane * share, dtype=jnp.int32)
    targets, weights = [], []
    for d in range(z_count):
        here = info
        if d:
            onward = [(s, (s + d * x_count) % sp_count) for s in range(sp_count)]
            here = lax.ppermute(info, "sp", onward)
        local = here[:, :top_count].astype(jnp.int32) - z * plane * capacity
        inside = (local >= 0) & (local < plane * capacity)
        target = local // capacity * share + d * capacity + local % capacity
        targets.append(jnp.where(inside, target, -1))
        weights.append(here[:, top_count:])
    target, weight = jnp.concatenate(targets), jnp.concatenate(weights)
    target_t = target.T
    select, weigh = False, 0.0
    for j in range(top_count):
        select = select | (slot_ids[:, None] == target_t[j][None, :])
        weigh = weigh + jnp.where(target[:, j, None] == slot_ids[None, :], weight[:, j, None], 0.0)
    select, weigh = select.astype(jnp.bfloat16), weigh.astype(jnp.bfloat16)
    wide = width // CHUNKS
    last = z_count - 1
    bf, f32 = jnp.bfloat16, jnp.float32
    vmem = pl.BlockSpec(memory_space=pltpu.VMEM)
    hbm = pl.BlockSpec(memory_space=pl.ANY)
    dma = pltpu.SemaphoreType.DMA
    slab = pltpu.VMEM((CHUNKS, plane * share, wide), bf)
    hop = pltpu.VMEM((CHUNKS, last, tok, wide), bf)
    return pl.pallas_call(
        lambda *refs: experts_kernel(z_count, x_count, tp_count, *refs),
        out_shape=jax.ShapeDtypeStruct((tok, width), bf),
        in_specs=[vmem] * 4 + [hbm] * 3,
        out_specs=vmem,
        scratch_shapes=[
            pltpu.VMEM((width, hidden), bf),
            pltpu.VMEM((width, hidden), bf),
            pltpu.VMEM((hidden, width), bf),
            hop,
            slab,
            slab,
            pltpu.VMEM((plane * share, hidden), f32),
            pltpu.VMEM((plane * share, hidden), f32),
            pltpu.VMEM((plane * share, hidden), bf),
            slab,
            slab,
            pltpu.VMEM((CHUNKS, z_count * tok, wide), f32),
            hop,
            hop,
            hop,
            hop,
            dma((3,)),
            dma((CHUNKS, 2, last)),
            dma((CHUNKS, last)),
            dma((CHUNKS, plane - 1)),
            dma((CHUNKS, plane - 1)),
            dma((CHUNKS, plane - 1)),
            dma((CHUNKS, plane - 1)),
            dma((CHUNKS, 2, last)),
            dma((CHUNKS, 2, last)),
        ],
        compiler_params=pltpu.CompilerParams(
            collective_id=0, has_side_effects=True, vmem_limit_bytes=65000 * 1024
        ),
        name="experts",
    )(normed, resid, select, weigh, gate, up, down)


def body(
    stream,
    projected,
    segments,
    group_weight,
    group_scale,
    out_weight,
    ffn_gain,
    routes,
    route_weights,
    expert_gate,
    expert_up,
    expert_down,
):
    mixed = pool(projected, segments, group_weight.shape[1])
    resid, normed = mixer(mixed, stream, group_weight, group_scale, out_weight, ffn_gain)
    return run_experts(
        normed, resid, routes, route_weights, expert_gate[0], expert_up[0], expert_down[0]
    )


def solution(mesh):
    in_specs = (
        P(("sp", "tp"), None),
        P("sp", "tp"),
        P("sp"),
        P(),
        P(),
        P(),
        P(),
        P(("sp", "tp"), None),
        P(("sp", "tp"), None),
        P(("sp", "tp"), None, None),
        P(("sp", "tp"), None, None),
        P(("sp", "tp"), None, None),
    )
    out_specs = P(("sp", "tp"), None)
    return jax.shard_map(body, mesh=mesh, in_specs=in_specs, out_specs=out_specs, check_vma=False)
```

profile of v0, /device:TPU:0, one launch (start us, length us, event | category | flops | bytes accessed | tf_op | source)
XLA Modules:
  0.0 173.1 jit_solution(7747552964149716530)
XLA Ops:
  0.0 0.7 convert_reduce_fusion
  0.7 0.1 fusion.27
  0.8 0.7 select_reduce_fusion
  1.6 0.7 fusion.30
  2.3 0.7 pad_maximum_fusion.1
  3.0 5.1 %collective-permute-start.4 = (f32[128,8]{0,1:T(8,128)S(1)}, f32[128,8]{0,1:T(8,128)S(1)}, u32[]{:S(2)}, u32[]{:S(2)}) collective-permute-start(f32[128,8]{0,1:T(8,128)S(1)} %pad_maximum_fusion.1), channel_id=1, source_target_pairs={{0,24},{4,28},{8,0},{12,4},{16,8},{20,12},{24,16},{28,20},{1,25},{... | collective-permute-start | bytes 12296 | tf_op jit(solution)/shard_map/ppermute | solution.py:437
  8.0 0.0 collective-permute-start.3
  8.1 1.0 collective-permute-start.2
  9.1 0.8 slice.85
  9.8 3.4 %collective-permute-start.1 = (s32[16]{0:T(128)S(1)}, s32[16]{0:T(128)S(1)}, u32[]{:S(2)}, u32[]{:S(2)}) collective-permute-start(s32[16]{0:T(128)S(1)} %slice.85), channel_id=1, source_target_pairs={{0,4},{4,8},{8,12},{12,16},{16,20},{20,24},{24,28},{1,5},{5,9},{9,... | collective-permute-start | bytes 200 | tf_op jit(solution)/shard_map/ppermute | solution.py:39
  13.2 0.7 slice.84
  13.9 4.3 %collective-permute-start = (bf16[16,512]{1,0:T(8,128)(2,1)S(1)}, bf16[16,512]{1,0:T(8,128)(2,1)S(1)}, u32[]{:S(2)}, u32[]{:S(2)}) collective-permute-start(bf16[16,512]{1,0:T(8,128)(2,1)S(1)} %slice.84), channel_id=1, source_target_pairs={{0,4},{4,8},{8,12},{12,16},{16,20},{20,24},{24,28},{1,5},{5,9},{9,... | collective-permute-start | bytes 49160 | tf_op jit(solution)/shard_map/ppermute | solution.py:38
  18.3 0.0 collective-permute-done.1
  18.3 0.8 pad_add_fusion.1
  19.1 0.0 collective-permute-done.4
  19.1 0.0 collective-permute-done.3
  19.1 0.0 collective-permute-done.2
  19.2 0.7 pad_maximum_fusion
  19.9 1.5 fusion.4.refs_2_
  21.4 0.0 collective-permute-done.refs_0_
  21.4 0.0 copy-start.2
  21.4 0.8 broadcast_in_dim.82.refs_2_
  22.3 0.0 copy-done.2
  22.3 3.3 %pool.1 = bf16[512,512]{1,0:T(8,128)(2,1)} custom-call(bf16[16,512]{1,0:T(8,128)(2,1)} %copy-done.2, bf16[512,512]{1,0:T(8,128)(2,1)} %refs_1_.1, s32[528,128]{1,0:T(8,128)} %broadcast_in_dim.82.refs_2_), custom_call_target="tpu_custom_call" | custom-call | tf_op jit(solution)/shard_map/pool/pallas_call | solution.py:43
  25.5 0.0 copy-start
  25.5 2.2 %copy.18 = bf16[4,128,512]{1,2,0:T(8,128)(2,1)} copy(bf16[4,128,512]{2,1,0:T(8,128)(2,1)} %bitcast.42) | data formatting | bytes 1048576 | tf_op jit(solution)/shard_map/all_to_all | solution.py:68
  27.7 3.5 %all-to-all-start = ((bf16[4,128,512]{1,2,0:T(8,128)(2,1)}), bf16[4,128,512]{1,2,0:T(8,128)(2,1)S(1)}, u32[]{:S(2)}, u32[]{:S(2)}) async-start(bf16[4,128,512]{1,2,0:T(8,128)(2,1)} %copy.18), calls=%async_computation | async-start | bytes 1048576 | tf_op jit(solution)/shard_map/all_to_all | solution.py:68
  31.2 1.7 add_convert_fusion.refs_3_
  32.9 7.1 %all-to-all-done = bf16[4,128,512]{1,2,0:T(8,128)(2,1)S(1)} async-done(((bf16[4,128,512]{1,2,0:T(8,128)(2,1)}), bf16[4,128,512]{1,2,0:T(8,128)(2,1)S(1)}, u32[]{:S(2)}, u32[]{:S(2)}) %all-to-all-start) | async-done | bytes 524320 | tf_op jit(solution)/shard_map/all_to_all | solution.py:68
  40.0 0.0 copy-done
  40.0 0.2 fusion.10
  40.2 0.0 copy-start.4
  40.3 0.0 copy-start.5
  40.3 0.2 fusion.12
  40.5 0.3 fusion.14
  40.8 0.3 fusion.16
  41.0 0.3 copy-done.4
  41.3 0.0 copy-done.5
  41.3 0.0 copy-start.3
  41.3 4.9 %fusion.5 = (f32[128]{0:T(128)S(1)}, bf16[128,2048]{1,0:T(8,128)(2,1)S(1)}) fusion(bf16[2048,2048]{1,0:T(8,128)(2,1)} %param.17, f32[128,512]{1,0:T(8,128)S(1)} %fusion.10, f32[128,512]{1,0:T(8,128)S(1)} %fusion.12, f32[128,512]{1,0:T(8,128)S(1)} %fusion.14, f32[128,512]{1,0:T(8,128)S(1)} %fusion.16, f32[2048]{0:T(1024)S(1)} %copy-done.5, ...), kind=kOutput, calls=%fused_computation.17 | convolution fusion | flops 1076625280 | bytes 10494464 | tf_op jit(solution)/shard_map/dot_general | solution.py:82
  46.2 0.0 copy-start.1
  46.2 0.8 copy-done.1
  47.0 0.0 copy-done.3
  47.0 1.0 fusion.7.refs_0_
  47.9 123.3 %experts.1 = bf16[128,2048]{1,0:T(8,128)(2,1)} custom-call(bf16[128,2048]{1,0:T(8,128)(2,1)} %fusion.7.refs_0_, bf16[128,2048]{1,0:T(8,128)(2,1)} %copy-done.1, bf16[768,512]{1,0:T(8,128)(2,1)} %fusion.4.refs_2_, bf16[512,768]{1,0:T(8,128)(2,1)} %add_convert_fusion.refs_3_, bf16[2048,1024]{1,0:T(8,128)(2,1)} %bitcast.35, bf16[2048,1024]{1,0:T(8,128)(2,1)} %bitcast.36, ...), custom_call_target="tpu_custom_call" | custom-call | tf_op jit(solution)/shard_map/experts/pallas_call | solution.py:458
  171.2 1.9 %copy.20 = bf16[128,2048]{1,0:T(8,128)(2,1)} copy(bf16[128,2048]{1,0:T(8,128)(2,1)} %experts.1) | data formatting | bytes 1048576
  (12 shorter events, 0.1 us)
Async XLA Ops:
  3.0 16.1 %collective-permute-start.4 = (f32[128,8]{0,1:T(8,128)S(1)}, f32[128,8]{0,1:T(8,128)S(1)}, u32[]{:S(2)}, u32[]{:S(2)}) collective-permute-start(f32[128,8]{0,1:T(8,128)S(1)} %pad_maximum_fusion.1), channel_id=1, source_target_pairs={{0,24},{4,28},{8,0},{12,4},{16,8},{20,12},{24,16},{28,20},{1,25},{... | collective-permute-start | bytes 12296 | tf_op jit(solution)/shard_map/ppermute | solution.py:437
  8.0 11.0 %collective-permute-start.3 = (f32[128,8]{0,1:T(8,128)S(1)}, f32[128,8]{0,1:T(8,128)S(1)}, u32[]{:S(2)}, u32[]{:S(2)}) collective-permute-start(f32[128,8]{0,1:T(8,128)S(1)} %pad_maximum_fusion.1), channel_id=1, source_target_pairs={{0,16},{4,20},{8,24},{12,28},{16,0},{20,4},{24,8},{28,12},{1,17},{... | collective-permute-start | bytes 12296 | tf_op jit(solution)/shard_map/ppermute | solution.py:437
  8.1 11.1 %collective-permute-start.2 = (f32[128,8]{0,1:T(8,128)S(1)}, f32[128,8]{0,1:T(8,128)S(1)}, u32[]{:S(2)}, u32[]{:S(2)}) collective-permute-start(f32[128,8]{0,1:T(8,128)S(1)} %pad_maximum_fusion.1), channel_id=1, source_target_pairs={{0,8},{4,12},{8,16},{12,20},{16,24},{20,28},{24,0},{28,4},{1,9},{5... | collective-permute-start | bytes 12296 | tf_op jit(solution)/shard_map/ppermute | solution.py:437
  9.8 8.5 %collective-permute-start.1 = (s32[16]{0:T(128)S(1)}, s32[16]{0:T(128)S(1)}, u32[]{:S(2)}, u32[]{:S(2)}) collective-permute-start(s32[16]{0:T(128)S(1)} %slice.85), channel_id=1, source_target_pairs={{0,4},{4,8},{8,12},{12,16},{16,20},{20,24},{24,28},{1,5},{5,9},{9,... | collective-permute-start | bytes 200 | tf_op jit(solution)/shard_map/ppermute | solution.py:39
  13.9 7.5 %collective-permute-start = (bf16[16,512]{1,0:T(8,128)(2,1)S(1)}, bf16[16,512]{1,0:T(8,128)(2,1)S(1)}, u32[]{:S(2)}, u32[]{:S(2)}) collective-permute-start(bf16[16,512]{1,0:T(8,128)(2,1)S(1)} %slice.84), channel_id=1, source_target_pairs={{0,4},{4,8},{8,12},{12,16},{16,20},{20,24},{24,28},{1,5},{5,9},{9,... | collective-permute-start | bytes 49160 | tf_op jit(solution)/shard_map/ppermute | solution.py:38
  21.4 0.9 copy-start.2
  25.5 14.5 %copy-start = (bf16[4,512,512]{2,1,0:T(8,128)(2,1)S(1)}, bf16[4,512,512]{2,1,0:T(8,128)(2,1)}, u32[]{:S(2)}) copy-start(bf16[4,512,512]{2,1,0:T(8,128)(2,1)} %param.15) | copy-start | bytes 6291460
  27.7 12.3 %all-to-all-start = ((bf16[4,128,512]{1,2,0:T(8,128)(2,1)}), bf16[4,128,512]{1,2,0:T(8,128)(2,1)S(1)}, u32[]{:S(2)}, u32[]{:S(2)}) async-start(bf16[4,128,512]{1,2,0:T(8,128)(2,1)} %copy.18), calls=%async_computation | async-start | bytes 1048576 | tf_op jit(solution)/shard_map/all_to_all | solution.py:68
  40.2 1.0 copy-start.4
  40.3 1.0 copy-start.5
  41.3 5.7 %copy-start.3 = (f32[2048]{0:T(1024)S(1)}, f32[2048]{0:T(1024)}, u32[]{:S(2)}) copy-start(f32[2048]{0:T(1024)} %param.18) | copy-start | bytes 24580
  46.2 0.8 copy-start.1
where the time goes:
time: 174 us; the launch traced here: 173 us
  Pallas kernels  127 us (73%)
  starting transfers between devices  17.3 us (10%)
  other arithmetic  8.53 us (5%)
  local copies, waits for them, and re-layouts  7.5 us (4%)
  waiting for transfers between devices  7.08 us (4%)
  matrix products  5.99 us (3%)
    pallas_call x1, Pallas kernels, run_experts(): pl.pallas_call(lambda *refs: experts_kernel(z_count, x_count, tp_count, *...  123 us
    all_to_all x1, waiting for transfers between devices, mixer(): lax.all_to_all(mixed, 'tp', split_axis=0, concat_axis=1, tiled=True)  7.06 us
    ppermute x3, starting transfers between devices, run_experts(): here = lax.ppermute(info, 'sp', onward)  6.09 us
    dot_general x1, matrix products, mixer(): mixer_out = jnp.dot(scaled, out_weight, preferred_element_type=jnp.float32)  4.85 us
    ppermute x1, starting transfers between devices, pool(): halo = lax.ppermute(projected[row_count - longest_window:], 'sp', onward)  4.34 us
  transfers between devices with their start and end apart: 6, of which 1 were waited for; matrix products, arithmetic and copies ran while one was open for 4% of the time, Pallas kernels for 0%

commit v1 on v0

v1 whole, which is shorter than its diff:
```python
import jax
import jax.numpy as jnp
from jax import lax
from jax.experimental import pallas as pl
from jax.experimental.pallas import tpu as pltpu
from jax.sharding import PartitionSpec as P

GROUPS = 4
CHUNKS = 8
REACH = 2
AHEAD = 2

norm_eps = 1e-05
clamp_limit = 7.0
sigmoid_alpha = 1.702
longest_window = 16


def layer_kernel(
    x_count,
    z_count,
    tp_count,
    capacity,
    share,
    routes_hbm,
    weights_hbm,
    docs_hbm,
    scale_hbm,
    gain_hbm,
    stream_hbm,
    proj_hbm,
    group_hbm,
    outw_hbm,
    gate_hbm,
    up_hbm,
    down_hbm,
    out_hbm,
    routes,
    weights,
    docs,
    prev_docs,
    scale,
    gain,
    stream,
    proj,
    group_ref,
    outw_ref,
    gate_ref,
    up_ref,
    down_ref,
    docs_col,
    mixed,
    gathered,
    scaled,
    squares,
    info,
    column,
    select,
    weigh,
    outgoing,
    rows,
    acc,
    activated,
    returned,
    sums_out,
    sums_in,
    sums_fwd,
    out_ref,
    load_sem,
    out_sem,
    halo_send,
    halo_recv,
    mix_send,
    mix_recv,
    info_send,
    info_recv,
    col_send,
    col_recv,
    plane_send,
    plane_recv,
    back_send,
    back_recv,
    sum_send,
    sum_recv,
    fwd_recv,
):
    sp, tp = lax.axis_index("sp"), lax.axis_index("tp")
    sp_count = x_count * z_count
    z, x = lax.div(sp, x_count), lax.rem(sp, x_count)
    plane = x_count * tp_count
    place = x * tp_count + tp
    tok, width = stream.shape
    channels = proj.shape[1]
    row_count = tok * tp_count
    group_width = group_ref.shape[1]
    top_count = routes.shape[0]
    hidden = gate_ref.shape[1]
    wide = width // CHUNKS
    tiles = hidden // wide
    halo = longest_window
    last = z_count - 1
    slot_count = plane * share
    first_row, last_row = sp > 0, sp < sp_count - 1

    def at_z(step):
        return {"sp": sp + step * x_count, "tp": tp}

    def at_plane(other):
        return {"sp": z * x_count + lax.div(other, tp_count), "tp": lax.rem(other, tp_count)}

    def remote(src, dst, send, recv, device):
        return pltpu.make_async_remote_copy(
            src_ref=src,
            dst_ref=dst,
            send_sem=send,
            recv_sem=recv,
            device_id=device,
            device_id_type=pl.DeviceIdType.MESH,
        )

    def cols_of(k):
        return pl.ds(pl.multiple_of(k * wide, wide), wide)

    def share_of(i):
        return pl.ds(pl.multiple_of(i * share, share), share)

    def block_of(i):
        return pl.ds(pl.multiple_of(i * tok, tok), tok)

    def inside(d, sgn):
        return (z + d <= last) if sgn > 0 else (z >= d)

    def behind(d, sgn):
        return inside(d, -sgn)

    pairs = (
        (proj_hbm, proj.at[pl.ds(halo, row_count)]),
        (docs_hbm, docs),
        (routes_hbm, routes),
        (weights_hbm, weights),
        (group_hbm, group_ref),
        (scale_hbm, scale),
        (gain_hbm, gain),
        (stream_hbm, stream),
        (outw_hbm, outw_ref),
        (gate_hbm, gate_ref),
        (up_hbm, up_ref),
        (down_hbm, down_ref),
    )
    loads = [
        pltpu.make_async_copy(src, dst, load_sem.at[i]) for i, (src, dst) in enumerate(pairs)
    ]
    for load in loads[:8]:
        load.start()

    barrier = pltpu.get_barrier_semaphore()

    def greet(device):
        pl.semaphore_signal(barrier, inc=1, device_id=device, device_id_type=pl.DeviceIdType.MESH)

    pl.when(first_row)(lambda: greet({"sp": sp - 1, "tp": tp}))
    pl.when(last_row)(lambda: greet({"sp": sp + 1, "tp": tp}))

    @pl.loop(1, z_count)
    def _(i):
        greet({"sp": lax.rem(sp + i * x_count, sp_count), "tp": tp})

    @pl.loop(1, plane)
    def _(i):
        greet(at_plane(lax.rem(place + i, plane)))

    for load in loads[8:]:
        load.start()

    loads[2].wait()
    loads[3].wait()
    expert_count = plane * z_count
    expert_ids = lax.broadcasted_iota(jnp.int32, (expert_count, tok), 0)
    named = [
        (expert_ids == routes[j : j + 1, :]).astype(jnp.float32) for j in range(top_count)
    ]
    marks = sum(named[1:], named[0])
    earlier = lax.broadcasted_iota(jnp.int32, (tok, tok), 0) < lax.broadcasted_iota(
        jnp.int32, (tok, tok), 1
    )
    before = jnp.dot(
        marks.astype(jnp.bfloat16),
        jnp.where(earlier, 1.0, 0.0).astype(jnp.bfloat16),
        preferred_element_type=jnp.float32,
    )
    for j in range(top_count):
        rank = jnp.sum(named[j] * before, 0, keepdims=True)
        info[z, j : j + 1, :] = routes[j : j + 1, :].astype(jnp.float32) * share + rank
    info[z, top_count : 2 * top_count, :] = weights[...]

    loads[0].wait()
    loads[1].wait()
    pl.semaphore_wait(
        barrier,
        plane - 1 + last + first_row.astype(jnp.int32) + last_row.astype(jnp.int32),
    )

    def halo_rows(device):
        return remote(
            proj.at[pl.ds(row_count, halo)],
            proj.at[pl.ds(0, halo)],
            halo_send.at[0],
            halo_recv.at[0],
            device,
        )

    def halo_docs(device):
        return remote(docs, prev_docs, halo_send.at[1], halo_recv.at[1], device)

    onward = {"sp": sp + 1, "tp": tp}

    @pl.when(last_row)
    def _():
        halo_rows(onward).start()
        halo_docs(onward).start()

    def info_to(i):
        return remote(
            info.at[z],
            info.at[z],
            info_send.at[i - 1],
            info_recv.at[z],
            {"sp": lax.rem(sp + i * x_count, sp_count), "tp": tp},
        )

    def info_from(i):
        other = lax.rem(z + i, z_count)
        return remote(
            info.at[other],
            info.at[other],
            info_send.at[i - 1],
            info_recv.at[other],
            {"sp": lax.rem(sp + i * x_count, sp_count), "tp": tp},
        )

    @pl.loop(1, z_count)
    def _(i):
        info_to(i).start()

    def spread(row):
        return jnp.broadcast_to(row, (128, row.shape[1])).T

    values = docs[...].astype(jnp.float32)
    for r in range(tp_count):
        docs_col[pl.ds(halo + r * tok, tok), :] = spread(values[r : r + 1, :])
    channel = tp * channels + lax.broadcasted_iota(jnp.int32, (tok + halo, 128), 1)

    def pool_block(r):
        window = pl.ds(r * tok, tok + halo)
        here = docs_col[window, :]
        joins = [
            (here == pltpu.roll(here, 1 << k, 0)) & (channel >= k * group_width)
            for k in range(GROUPS)
        ]
        count = jnp.ones_like(here)
        for k in range(GROUPS):
            count = jnp.where(joins[k], count + pltpu.roll(count, 1 << k, 0), count)
        inverse = 1.0 / count
        for lane in range(0, channels, 128):
            cols = slice(lane, lane + 128)
            own = proj[window, cols].astype(jnp.float32)
            total = own
            for k in range(GROUPS):
                total = jnp.where(joins[k], total + pltpu.roll(total, 1 << k, 0), total)
            mixed[r, :, cols] = (total * inverse - own)[halo:].astype(jnp.bfloat16)

    def mix_to(r):
        return remote(
            mixed.at[r],
            gathered.at[tp],
            mix_send.at[r],
            mix_recv.at[tp],
            {"sp": sp, "tp": r},
        )

    def mix_from(r):
        return remote(
            mixed.at[r],
            gathered.at[r],
            mix_send.at[r],
            mix_recv.at[r],
            {"sp": sp, "tp": r},
        )

    for r in [*range(1, tp_count), 0]:
        if r == 0:

            @pl.when(first_row)
            def _():
                halo_rows(onward).wait_recv()
                halo_docs(onward).wait_recv()
                tail = prev_docs[tp_count - 1 : tp_count, :].astype(jnp.float32)
                docs_col[pl.ds(0, halo), :] = spread(tail)[tok - halo :]

            @pl.when(jnp.logical_not(first_row))
            def _():
                proj[pl.ds(0, halo), :] = jnp.zeros((halo, channels), proj.dtype)
                docs_col[pl.ds(0, halo), :] = jnp.full((halo, 128), -1.0, jnp.float32)

        pool_block(r)
        pl.when(tp != r)(lambda r=r: mix_to(r).start())

        @pl.when(tp == r)
        def _(r=r):
            gathered[r] = mixed[r]

    @pl.loop(1, z_count)
    def _(i):
        info_from(i).wait_recv()

    slot_rows = lax.broadcasted_iota(jnp.int32, (slot_count, tok), 0).astype(jnp.float32)
    slot_cols = lax.broadcasted_iota(jnp.int32, (tok, slot_count), 1).astype(jnp.float32)
    base = (z * slot_count).astype(jnp.float32)

    for s in range(z_count):
        theirs = info[s]
        local = theirs[:top_count] - base
        here = (local >= 0.0) & (local < float(slot_count))
        target = jnp.where(here, local + float(s * capacity), -1.0)
        both = jnp.concatenate([target, theirs[top_count:]], 0)
        turned = both.T
        picks = slot_rows == target[0:1, :]
        for j in range(1, top_count):
            picks = picks | (slot_rows == target[j : j + 1, :])
        select[:, s * tok : (s + 1) * tok] = jnp.where(picks, 1.0, 0.0).astype(jnp.bfloat16)
        share_out = jnp.where(
            slot_cols == turned[:, 0:1], turned[:, top_count : top_count + 1], 0.0
        )
        for j in range(1, top_count):
            share_out = jnp.where(
                slot_cols == turned[:, j : j + 1],
                turned[:, top_count + j : top_count + j + 1],
                share_out,
            )
        weigh[s * tok : (s + 1) * tok, :] = share_out.astype(jnp.bfloat16)

    for i in (4, 5, 6, 7, 8):
        loads[i].wait()
    for r in range(tp_count):
        pl.when(tp != r)(lambda r=r: mix_from(r).wait_recv())
    pieces = group_width // channels
    for g in range(GROUPS):
        grouped = jnp.zeros((tok, group_width), jnp.float32)
        for p in range(pieces):
            grouped += jnp.dot(
                gathered[g * pieces + p],
                group_ref[g, p * channels : (p + 1) * channels, :],
                preferred_element_type=jnp.float32,
            )
        cols = slice(g * group_width, (g + 1) * group_width)
        scaled[:, cols] = (grouped * scale[:, cols]).astype(jnp.bfloat16)
    squares[...] = jnp.zeros_like(squares)

    @pl.loop(0, CHUNKS)
    def _(k):
        cols = cols_of(k)
        mixer_out = jnp.dot(scaled[...], outw_ref[:, cols], preferred_element_type=jnp.float32)
        resid = (stream[:, cols].astype(jnp.float32) + mixer_out).astype(jnp.bfloat16)
        stream[:, cols] = resid
        resid = resid.astype(jnp.float32)
        for lane in range(0, wide, 128):
            part = resid[:, lane : lane + 128]
            squares[...] += part * part

    mean = jnp.sum(squares[...], -1, keepdims=True) * (1.0 / width)
    inverse = lax.rsqrt(mean + norm_eps)

    def own_to(k, d, sgn):
        return remote(
            column.at[k, block_of(z)],
            column.at[k, block_of(z)],
            col_send.at[k, 0 if sgn > 0 else 1, d - 1],
            col_recv.at[k, z],
            at_z(sgn * d),
        )

    def relay(k, d, sgn):
        origin = z - sgn * (d - 1)
        return remote(
            column.at[k, block_of(origin)],
            column.at[k, block_of(origin)],
            col_send.at[k, 0 if sgn > 0 else 1, d - 1],
            col_recv.at[k, origin],
            at_z(sgn),
        )

    def arrival(k, d, sgn):
        origin = z - sgn * d
        return remote(
            column.at[k, block_of(origin)],
            column.at[k, block_of(origin)],
            col_send.at[k, 0 if sgn > 0 else 1, d - 1],
            col_recv.at[k, origin],
            at_z(sgn),
        )

    def send_own(k):
        for d in range(min(REACH, last), 0, -1):
            for sgn in (1, -1):
                pl.when(inside(d, sgn))(lambda d=d, sgn=sgn: own_to(k, d, sgn).start())

    @pl.loop(0, CHUNKS)
    def _(k):
        cols = cols_of(k)
        values = stream[:, cols].astype(jnp.float32)
        column[k, block_of(z), :] = (values * inverse * gain[:, cols]).astype(jnp.bfloat16)
        pl.when(k < AHEAD)(lambda: send_own(k))

    def collect(k):
        for d in range(min(REACH, last), 0, -1):
            for sgn in (1, -1):

                @pl.when(behind(d, sgn))
                def _(d=d, sgn=sgn):
                    arrival(k, d, sgn).wait_recv()
                    if d == REACH and d < last:
                        pl.when(inside(1, sgn))(lambda: relay(k, d + 1, sgn).start())

        for d in range(REACH + 1, z_count):
            for sgn in (1, -1):

                @pl.when(behind(d, sgn))
                def _(d=d, sgn=sgn):
                    arrival(k, d, sgn).wait_recv()
                    if d < last:
                        pl.when(inside(1, sgn))(lambda: relay(k, d + 1, sgn).start())

    def to_expert(k, i):
        other = lax.rem(place + i, plane)
        return remote(
            outgoing.at[k, share_of(other)],
            rows.at[k, share_of(i)],
            plane_send.at[k, i - 1],
            plane_recv.at[k, i - 1],
            at_plane(other),
        )

    def dispatch(k):
        outgoing[k] = jnp.dot(
            select[...], column[k], preferred_element_type=jnp.float32
        ).astype(jnp.bfloat16)

        @pl.loop(1, plane)
        def _(i):
            to_expert(k, i).start()

        rows[k, pl.ds(0, share)] = outgoing[k, share_of(place)]

    def received(k):
        @pl.loop(1, plane)
        def _(i):
            to_expert(k, i).wait_recv()

    def tile_of(n):
        return pl.ds(pl.multiple_of(n * wide, wide), wide)

    def product(k, ref, n):
        return jnp.dot(rows[k], ref[cols_of(k), tile_of(n)], preferred_element_type=jnp.float32)

    def accumulate(k):
        received(k)

        @pl.when(k == 0)
        def _():
            loads[9].wait()
            loads[10].wait()

            @pl.loop(0, tiles)
            def _(n):
                acc[n, 0:slot_count] = product(0, gate_ref, n)
                acc[tiles + n, 0:slot_count] = product(0, up_ref, n)

        @pl.when(k > 0)
        def _():
            @pl.loop(0, tiles)
            def _(n):
                acc[n, 0:slot_count] += product(k, gate_ref, n)
                acc[tiles + n, 0:slot_count] += product(k, up_ref, n)

    @pl.loop(0, CHUNKS)
    def _(k):
        pl.when(k + AHEAD < CHUNKS)(lambda: send_own(k + AHEAD))
        collect(k)
        dispatch(k)
        pl.when(k > 0)(lambda: accumulate(k - 1))

    received(CHUNKS - 1)

    @pl.loop(0, tiles)
    def _(n):
        gate_value = acc[n, 0:slot_count] + product(CHUNKS - 1, gate_ref, n)
        up_value = acc[tiles + n, 0:slot_count] + product(CHUNKS - 1, up_ref, n)
        gated = jnp.minimum(gate_value, clamp_limit)
        linear = jnp.clip(up_value, -clamp_limit, clamp_limit)
        activated[:, tile_of(n)] = (
            gated * jax.nn.sigmoid(sigmoid_alpha * gated) * (linear + 1.0)
        ).astype(jnp.bfloat16)

    loads[11].wait()

    def to_relay(k, i):
        return remote(
            outgoing.at[k, share_of(i)],
            returned.at[k, share_of(place)],
            back_send.at[k, i - 1],
            back_recv.at[k, i - 1],
            at_plane(lax.rem(place + plane - i, plane)),
        )

    @pl.loop(0, CHUNKS)
    def _(k):
        @pl.loop(1, plane)
        def _(i):
            to_expert(k, i).wait_send()

        outgoing[k] = jnp.dot(
            activated[...], down_ref[:, cols_of(k)], preferred_element_type=jnp.float32
        ).astype(jnp.bfloat16)

        @pl.loop(1, plane)
        def _(i):
            to_relay(k, i).start()

        returned[k, share_of(place)] = outgoing[k, pl.ds(0, share)]

    def sum_to(k, d, sgn):
        target = z + sgn * d
        if d <= REACH:
            return remote(
                sums_out.at[k, target],
                sums_in.at[k, z],
                sum_send.at[k, target],
                sum_recv.at[k, z],
                at_z(sgn * d),
            )
        return remote(
            sums_out.at[k, target],
            sums_fwd.at[k, target],
            sum_send.at[k, target],
            fwd_recv.at[k, target],
            at_z(sgn),
        )

    def sum_from(k, d, sgn):
        origin = z - sgn * d
        return remote(
            sums_out.at[k, origin],
            sums_in.at[k, origin],
            sum_send.at[k, origin],
            sum_recv.at[k, origin],
            at_z(-sgn * d),
        )

    def forwarded(k, d, sgn):
        target = z + sgn * d
        return remote(
            sums_out.at[k, target],
            sums_fwd.at[k, target],
            sum_send.at[k, target],
            fwd_recv.at[k, target],
            at_z(-sgn),
        )

    def combine(k):
        @pl.loop(1, plane)
        def _(i):
            to_relay(k, i).wait_recv()

        acc[k, 0 : z_count * tok] = jnp.dot(
            weigh[...], returned[k], preferred_element_type=jnp.float32
        )
        for d in range(last, 0, -1):
            for sgn in (1, -1):

                def emit(d=d, sgn=sgn):
                    sums_out[k, z + sgn * d] = acc[k, block_of(z + sgn * d)].astype(jnp.bfloat16)
                    sum_to(k, d, sgn).start()

                if d < REACH:
                    pl.when(inside(d, sgn))(emit)
                else:
                    pl.when(inside(d, sgn) & jnp.logical_not(behind(1, sgn)))(emit)

    def pass_on(k):
        for d in range(last - 1, REACH - 1, -1):
            for sgn in (1, -1):

                @pl.when(inside(d, sgn) & behind(1, sgn))
                def _(d=d, sgn=sgn):
                    target = z + sgn * d
                    forwarded(k, d, sgn).wait_recv()
                    sums_out[k, target] = (
                        acc[k, block_of(target)] + sums_fwd[k, target].astype(jnp.float32)
                    ).astype(jnp.bfloat16)
                    sum_to(k, d, sgn).start()

    def put_out(k):
        return pltpu.make_async_copy(
            out_ref.at[:, cols_of(k)], out_hbm.at[:, cols_of(k)], out_sem.at[k]
        )

    def finish(k):
        own = block_of(z)
        for d in range(1, min(REACH, last) + 1):
            for sgn in (1, -1):

                @pl.when(behind(d, sgn))
                def _(d=d, sgn=sgn):
                    sum_from(k, d, sgn).wait_recv()
                    acc[k, own] += sums_in[k, z - sgn * d].astype(jnp.float32)

        out_ref[:, cols_of(k)] = (
            stream[:, cols_of(k)].astype(jnp.float32) + acc[k, own]
        ).astype(jnp.bfloat16)
        put_out(k).start()

    @pl.loop(0, CHUNKS)
    def _(k):
        combine(k)
        pl.when(k > 0)(lambda: pass_on(k - 1))
        pl.when(k > 1)(lambda: finish(k - 2))

    pass_on(CHUNKS - 1)
    finish(CHUNKS - 2)
    finish(CHUNKS - 1)

    @pl.when(last_row)
    def _():
        halo_rows(onward).wait_send()
        halo_docs(onward).wait_send()

    @pl.loop(1, z_count)
    def _(i):
        info_to(i).wait_send()

    for r in range(tp_count):
        pl.when(tp != r)(lambda r=r: mix_to(r).wait_send())

    @pl.loop(0, CHUNKS)
    def _(k):
        for d in range(1, z_count):
            for sgn in (1, -1):
                if d <= REACH:
                    pl.when(inside(d, sgn))(lambda d=d, sgn=sgn: own_to(k, d, sgn).wait_send())
                else:

                    @pl.when(behind(d - 1, sgn) & inside(1, sgn))
                    def _(d=d, sgn=sgn):
                        relay(k, d, sgn).wait_send()

                pl.when(inside(d, sgn))(lambda d=d, sgn=sgn: sum_to(k, d, sgn).wait_send())

        @pl.loop(1, plane)
        def _(i):
            to_relay(k, i).wait_send()

        put_out(k).wait()


def body(
    stream,
    projected,
    segments,
    group_weight,
    group_scale,
    out_weight,
    ffn_gain,
    routes,
    route_weights,
    expert_gate,
    expert_up,
    expert_down,
):
    tok, width = stream.shape
    row_count, channels = projected.shape
    sp_count, tp_count = lax.axis_size("sp"), lax.axis_size("tp")
    x_count = max(tp_count // 2, 1)
    z_count = sp_count // x_count
    plane = x_count * tp_count
    top_count = routes.shape[1]
    group_width = group_weight.shape[1]
    hidden = expert_gate.shape[2]
    capacity = 3 * tok * top_count // (2 * plane * z_count)
    share = -(-z_count * capacity // 16) * 16
    slots = plane * share
    wide = width // CHUNKS
    last = max(z_count - 1, 1)
    acc_shape = (max(2 * hidden // wide, CHUNKS), max(slots, z_count * tok), wide)
    bf, f32, i32 = jnp.bfloat16, jnp.float32, jnp.int32
    hbm = pl.BlockSpec(memory_space=pltpu.HBM)
    dma = pltpu.SemaphoreType.DMA
    vmem = pltpu.VMEM
    return pl.pallas_call(
        lambda *refs: layer_kernel(x_count, z_count, tp_count, capacity, share, *refs),
        out_shape=jax.ShapeDtypeStruct((tok, width), bf),
        in_specs=[hbm] * 12,
        out_specs=hbm,
        scratch_shapes=[
            vmem((top_count, tok), i32),
            vmem((top_count, tok), f32),
            vmem((tp_count, tok), i32),
            vmem((tp_count, tok), i32),
            vmem((1, width), f32),
            vmem((1, width), f32),
            vmem((tok, width), bf),
            vmem((longest_window + row_count, channels), bf),
            vmem(group_weight.shape, bf),
            vmem(out_weight.shape, bf),
            vmem((width, hidden), bf),
            vmem((width, hidden), bf),
            vmem((hidden, width), bf),
            vmem((longest_window + row_count, 128), f32),
            vmem((tp_count, tok, channels), bf),
            vmem((tp_count, tok, channels), bf),
            vmem((tok, width), bf),
            vmem((tok, 128), f32),
            vmem((z_count, 2 * top_count, tok), f32),
            vmem((CHUNKS, z_count * tok, wide), bf),
            vmem((slots, z_count * tok), bf),
            vmem((z_count * tok, slots), bf),
            vmem((CHUNKS, slots, wide), bf),
            vmem((CHUNKS, slots, wide), bf),
            vmem(acc_shape, f32),
            vmem((slots, hidden), bf),
            vmem((CHUNKS, slots, wide), bf),
            vmem((CHUNKS, z_count, tok, wide), bf),
            vmem((CHUNKS, z_count, tok, wide), bf),
            vmem((CHUNKS, z_count, tok, wide), bf),
            vmem((tok, width), bf),
            dma((12,)),
            dma((CHUNKS,)),
            dma((2,)),
            dma((2,)),
            dma((tp_count,)),
            dma((tp_count,)),
            dma((last,)),
            dma((z_count,)),
            dma((CHUNKS, 2, last)),
            dma((CHUNKS, z_count)),
            dma((CHUNKS, plane - 1)),
            dma((CHUNKS, plane - 1)),
            dma((CHUNKS, plane - 1)),
            dma((CHUNKS, plane - 1)),
            dma((CHUNKS, z_count)),
            dma((CHUNKS, z_count)),
            dma((CHUNKS, z_count)),
        ],
        compiler_params=pltpu.CompilerParams(
            collective_id=0, has_side_effects=True, vmem_limit_bytes=65000 * 1024
        ),
        name="layer",
    )(
        routes.T,
        route_weights.T,
        segments.reshape(tp_count, tok),
        group_scale.reshape(1, width),
        ffn_gain.reshape(1, width),
        stream,
        projected,
        group_weight,
        out_weight,
        expert_gate[0],
        expert_up[0],
        expert_down[0],
    )


def solution(mesh):
    in_specs = (
        P(("sp", "tp"), None),
        P("sp", "tp"),
        P("sp"),
        P(),
        P(),
        P(),
        P(),
        P(("sp", "tp"), None),
        P(("sp", "tp"), None),
        P(("sp", "tp"), None, None),
        P(("sp", "tp"), None, None),
        P(("sp", "tp"), None, None),
    )
    out_specs = P(("sp", "tp"), None)
    return jax.shard_map(body, mesh=mesh, in_specs=in_specs, out_specs=out_specs, check_vma=False)
```

time: 174 us -> 121 us (0.70)
  starting transfers between devices: 17.3 us -> 0 us
  other arithmetic: 8.53 us -> 0 us
  Pallas kernels: 127 us -> 119 us
  waiting for transfers between devices: 7.08 us -> 0 us
  matrix products: 5.99 us -> 0 us
  local copies, waits for them, and re-layouts: 7.5 us -> 1.88 us
    ppermute x5 -> x0, starting transfers between devices: 13.8 us -> none  [the longest x3 6.09 us: run_experts(): here = lax.ppermute(info, 'sp', onward)]
    pallas_call x2 -> x1, Pallas kernels: 127 us -> 119 us  [body(): pl.pallas_call(lambda *refs: layer_kernel(x_count, z_count, tp_count, cap...]
    all_to_all x1 -> x0, waiting for transfers between devices: 7.06 us -> none  [mixer(): lax.all_to_all(mixed, 'tp', split_axis=0, concat_axis=1, tiled=True)]
    dot_general x6 -> x0, matrix products: 5.99 us -> none  [the longest x1 4.85 us: mixer(): mixer_out = jnp.dot(scaled, out_weight, preferred_element_type=jnp.float32)]
    convert_element_type x3 -> x0, other arithmetic: 4.19 us -> none  [the longest x2 3.21 us: run_experts(): select, weigh = (select.astype(jnp.bfloat16), weigh.astype(jnp.bfloat16))]
    all_to_all x1 -> x0, starting transfers between devices: 3.47 us -> none  [mixer(): lax.all_to_all(mixed, 'tp', split_axis=0, concat_axis=1, tiled=True)]
    all_to_all x1 -> x0, local copies, waits for them, and re-layouts: 2.2 us -> none  [mixer(): lax.all_to_all(mixed, 'tp', split_axis=0, concat_axis=1, tiled=True)]
    concatenate x4 -> x0, other arithmetic: 2.14 us -> none  [the longest x1 0.76 us: pool(): docs = jnp.concatenate([halo_docs, segments])]
  transfers between devices with their start and end apart: 6 -> 0, of which waited for: 1 -> 0; matrix products, arithmetic and copies ran while one was open for 4% -> 0% of each run, Pallas kernels for 0% -> 0%
where the time goes in v1:
time: 121 us
  Pallas kernels  119 us (98%)
  local copies, waits for them, and re-layouts  1.88 us (2%)
    pallas_call x1, Pallas kernels, body(): pl.pallas_call(lambda *refs: layer_kernel(x_count, z_count, tp_count, cap...  119 us

profile of v1, /device:TPU:0, one launch (start us, length us, event | category | flops | bytes accessed | tf_op | source)
XLA Modules:
  0.0 121.0 jit_solution(12980279580858242054)
XLA Ops:
  0.0 119.1 %layer.1 = bf16[128,2048]{1,0:T(8,128)(2,1)} custom-call(s32[4,128]{1,0:T(4,128)} %bitcast.13, f32[4,128]{1,0:T(4,128)} %bitcast.14, s32[4,128]{1,0:T(4,128)} %bitcast.15, f32[1,2048]{1,0:T(1,128)} %bitcast.11, f32[1,2048]{1,0:T(1,128)} %bitcast.12, bf16[128,2048]{1,0:T(8,128)(2,1)} %refs_5_.1, bf16[512,512]{1,0:T(8,128)(2,1)} %refs_6_.1, ...), custom_call_target="tpu_custom_call" | custom-call | tf_op jit(solution)/shard_map/layer/pallas_call | solution.py:698
  119.1 1.9 %copy.14 = bf16[128,2048]{1,0:T(8,128)(2,1)} copy(bf16[128,2048]{1,0:T(8,128)(2,1)} %layer.1) | data formatting | bytes 1048576
